TPU v7x, 32 devices: a whole 2x2x4 slice. The times are simulated.
32 devices in a mesh: sp: 4 (over y, core), dp: 8 (over z, x).
Axes of the slice: x: 2, y: 2, z: 4, core: 2. Of those that a mesh axis runs over, the one named last changes fastest.
Arguments:
- stream: bfloat16 [8, 512, 2064], P('dp', 'sp'), may hold values from -6 to 6
- mix_gain: float32 [2064], replicated, may hold values from 0.1 to 1.9
- query_weight: bfloat16 [2064, 2048], P('dp'), may hold values from -0.125 to 0.125
- query_gain: float32 [128], replicated, may hold values from 0.1 to 1.9
- keys: bfloat16 [8, 512, 512], P('dp', 'sp'), may hold values from -6 to 6
- key_gain: float32 [128], replicated, may hold values from 0.1 to 1.9
- values: bfloat16 [8, 512, 512], P('dp', 'sp'), may hold values from -48 to 48
- stick_offset: float32 [16], replicated, may hold values from -8.5 to -7, as said below
Outputs:
- attended: bfloat16 [8, 512, 2048], P('dp', 'sp')
Inputs may be any that keep to these rules, and one draw needn't show every extreme that they name: `stick_offset`: one offset for each query head, added to all of that head's scores.
All inputs are finite; a program needn't handle non-finite values.
Results may differ from a plain program's by a relative error of at most 0.012.
Values may be sent and summed in bfloat16 or wider, within the bound.
A program may use at most 64 MiB of HBM per device.

v0:
```python
import math
import jax
import jax.numpy as jnp
from jax import lax
from jax.sharding import PartitionSpec as P

norm_eps = 1e-06
row_block = 256
key_block = 128


def rms_scaled(inputs, gain):
    wide = inputs.astype(jnp.float32)
    scaled = wide * lax.rsqrt(jnp.mean(wide * wide, axis=-1, keepdims=True) + norm_eps) * gain
    return scaled.astype(jnp.bfloat16)


def stick_weights(scores, first_row):
    heads_here = scores.shape[0]
    rows_here = scores.shape[1]
    keys_here = scores.shape[2]
    width = math.gcd(keys_here, key_block)
    blocks_here = keys_here // width
    query_pos = first_row + jnp.arange(rows_here, dtype=jnp.int32)
    key_pos = jnp.arange(keys_here, dtype=jnp.int32)
    causal = key_pos[None, :] < query_pos[:, None]
    log_keep = jnp.where(causal, jax.nn.log_sigmoid(-scores), 0.0)
    pieces = log_keep.reshape(heads_here, rows_here, blocks_here, width)
    inner = jnp.arange(width, dtype=jnp.int32)
    upper = (inner[:, None] > inner[None, :]).astype(jnp.float32)
    local = jnp.einsum("hqbk,kj->hqbj", pieces, upper, precision=lax.Precision.HIGHEST)
    totals = jnp.sum(pieces, axis=3)
    later = lax.cumsum(totals, axis=2, reverse=True) - totals
    tail = (local + later[:, :, :, None]).reshape(heads_here, rows_here, keys_here)
    return jnp.where(causal, jnp.exp(jax.nn.log_sigmoid(scores) + tail), 0.0)


def body(stream, mix_gain, query_weight, query_gain, keys, key_gain, values, stick_offset):
    sp_count = lax.axis_size("sp")
    sp_index = lax.axis_index("sp")
    stream_rows = stream[0]
    tokens_dev = stream_rows.shape[0]
    head_width = query_gain.shape[0]
    heads_all = stick_offset.shape[0]
    heads_dev = heads_all // sp_count
    kv_count = keys.shape[2] // head_width
    group_size = sp_count // kv_count
    seq_length = tokens_dev * sp_count
    stacked = jnp.stack((keys[0], values[0]), axis=1).reshape(tokens_dev, 2, kv_count, head_width)
    copied = jnp.repeat(stacked, group_size, axis=2)
    arrived = lax.all_to_all(copied, "sp", split_axis=2, concat_axis=0, tiled=True)
    key_value = arrived[:, :, 0, :]
    normed = rms_scaled(stream_rows, mix_gain)
    columns = lax.dynamic_slice_in_dim(
        query_weight, sp_index * (heads_dev * head_width), heads_dev * head_width, 1
    )
    gathered = lax.all_gather(columns, "dp", axis=0, tiled=True)
    queries = jnp.dot(
        lax.all_gather(normed, "sp", axis=0, tiled=True),
        gathered,
        preferred_element_type=jnp.float32,
    ).astype(jnp.bfloat16)
    queries = lax.optimization_barrier(queries)
    mine = rms_scaled(queries.reshape(seq_length, heads_dev, head_width), query_gain)
    key_heads = rms_scaled(key_value[:, 0], key_gain)
    value_rows = key_value[:, 1]
    offsets = lax.dynamic_slice_in_dim(stick_offset, sp_index * heads_dev, heads_dev)
    block = math.gcd(seq_length, row_block)
    outputs = []
    for block_id in range(seq_length // block):
        first = block_id * block
        finish = first + block
        scores = jnp.einsum(
            "qhd,kd->hqk",
            mine[first:finish],
            key_heads[:finish],
            preferred_element_type=jnp.float32,
        )
        scores = scores * head_width ** (-0.5) + offsets[:, None, None]
        weights = stick_weights(scores, first).astype(jnp.bfloat16)
        outputs.append(
            jnp.einsum(
                "hqk,kd->qhd", weights, value_rows[:finish], preferred_element_type=jnp.float32
            )
        )
    attended = (
        jnp.concatenate(outputs, axis=0)
        .reshape(seq_length, heads_dev * head_width)
        .astype(jnp.bfloat16)
    )
    returned = lax.all_to_all(attended, "sp", split_axis=0, concat_axis=1, tiled=True)
    return returned[None]


def solution(mesh):
    return jax.shard_map(
        body,
        mesh=mesh,
        in_specs=(
            P("dp", "sp", None),
            P(),
            P("dp", None),
            P(),
            P("dp", "sp", None),
            P(),
            P("dp", "sp", None),
            P(),
        ),
        out_specs=P("dp", "sp", None),
        check_vma=False,
    )
```

profile of v0, /device:TPU:0, one launch (start us, length us, event | category | flops | bytes accessed | tf_op | source)
XLA Modules:
  0.0 124.1 jit_solution(3568556610034957392)
XLA Ops:
  6.5 0.0 copy-start
  6.5 0.0 copy-start.7
  6.5 0.0 copy-start.8
  6.5 0.0 all-gather.6.cloned.1.call-start
  6.6 1.2 copy-done
  7.8 0.7 dynamic-slice_bitcast_fusion
  8.5 0.0 all-gather.6.cloned.1.call-update
  8.5 0.0 copy-start.12
  8.5 0.0 all-gather.4.cloned.1.call-start
  8.6 1.3 %fusion.15 = f32[128]{0:T(128)S(1)} fusion(bf16[1,128,2064]{1,2,0:T(8,128)(2,1)} %param.8), kind=kLoop, calls=%fused_computation.31 | loop fusion | flops 792448 | bytes 528896 | tf_op jit(solution)/shard_map/reduce_sum | solution.py:14
  9.9 0.0 copy-start.10
  9.9 2.2 %fusion.17 = bf16[128,2064]{0,1:T(8,128)(2,1)} fusion(bf16[1,128,2064]{1,2,0:T(8,128)(2,1)} %param.8, f32[2064]{0:T(1024)} %param.9, f32[128]{0:T(128)S(1)} %add_rsqrt_fusion.2), kind=kLoop, calls=%fused_computation.33 | loop fusion | flops 1056768 | bytes 1065536 | tf_op jit(solution)/shard_map/convert_element_type | solution.py:15
  12.1 0.0 all-gather.4.cloned.1.call-update
  12.2 0.0 copy-done.7
  12.2 0.1 copy.54
  12.3 0.0 copy-done.8
  12.3 0.1 copy.55
  12.5 0.9 copy.56
  13.3 4.3 %all-to-all-start = ((bf16[128,2,4,128]{3,0,1,2:T(8,128)(2,1)}), bf16[128,2,4,128]{3,0,1,2:T(8,128)(2,1)S(1)}, u32[]{:S(2)}, u32[]{:S(2)}) async-start(bf16[128,2,4,128]{3,0,1,2:T(8,128)(2,1)} %copy.56), calls=%async_computation | async-start | bytes 524288 | tf_op jit(solution)/shard_map/all_to_all | solution.py:51
  17.6 0.0 copy-done.12
  17.6 0.1 dynamic_slice.7
  17.7 0.7 iota_compare_fusion
  18.5 5.2 %all-to-all-done = bf16[128,2,4,128]{3,0,1,2:T(8,128)(2,1)S(1)} async-done(((bf16[128,2,4,128]{3,0,1,2:T(8,128)(2,1)}), bf16[128,2,4,128]{3,0,1,2:T(8,128)(2,1)S(1)}, u32[]{:S(2)}, u32[]{:S(2)}) %all-to-all-start) | async-done | bytes 262176 | tf_op jit(solution)/shard_map/all_to_all | solution.py:51
  23.6 0.1 fusion.27
  23.8 0.0 copy-done.10
  23.8 0.8 fusion.29
  24.6 37.5 %all-gather.6.cloned.1.call-done = bf16[8,258,512]{2,1,0:T(8,128)(2,1)} async-done(((bf16[1,258,512]{2,1,0:T(8,128)(2,1)}), bf16[8,258,512]{2,1,0:T(8,128)(2,1)}) %all-gather.6.cloned.1.call-update) | async-done | bytes 2113552 | tf_op jit(solution)/shard_map/all_gather | solution.py:57
  62.1 1.9 %reshape.90 = bf16[2064,512]{1,0:T(8,128)(2,1)S(1)} reshape(bf16[8,258,512]{2,1,0:T(8,128)(2,1)} %all-gather.6.cloned.1.call-done) | data formatting | bytes 4227072
  63.9 21.1 %all-gather.4.cloned.1.call-done = bf16[512,2064]{0,1:T(8,128)(2,1)} async-done(((bf16[128,2064]{0,1:T(8,128)(2,1)}), bf16[512,2064]{0,1:T(8,128)(2,1)}) %all-gather.4.cloned.1.call-update) | async-done | bytes 2113552 | tf_op jit(solution)/shard_map/all_gather | solution.py:59
  85.1 3.8 %convolution_convert_fusion = bf16[512,512]{1,0:T(8,128)(2,1)} fusion(bf16[512,2064]{0,1:T(8,128)(2,1)} %all-gather.4.cloned.1.call-done, bf16[2064,512]{1,0:T(8,128)(2,1)S(1)} %reshape.90), kind=kOutput, calls=%fused_computation.26 | convolution fusion | flops 1082392576 | bytes 4751360 | tf_op jit(solution)/shard_map/dot_general | solution.py:58
  88.9 0.0 copy-start.1
  88.9 0.0 copy-start.11
  88.9 1.4 %reshape.88 = f32[512,4,128]{2,1,0:T(4,128)S(1)} reshape(bf16[512,512]{1,0:T(8,128)(2,1)} %convolution_convert_fusion) | data formatting | bytes 1572864 | tf_op jit(solution)/shard_map/convert_element_type | solution.py:13
  90.3 0.6 multiply_reduce_fusion
  90.9 0.1 copy.58
  91.1 0.0 copy-done.1
  91.1 0.0 copy-done.11
  91.1 0.3 fusion.26
  91.4 0.0 copy-start.5
  91.4 0.8 copy-done.5
  92.2 1.8 %bitcast_reduce_fusion.1 = (f32[4,256,2]{1,2,0:T(2,128)S(1)}, f32[4,256,256]{1,2,0:T(8,128)S(1)}, f32[4,256,256]{1,2,0:T(8,128)S(1)}) fusion(pred[256,256]{0,1:T(8,128)(4,1)S(1)} %iota_compare_fusion.1, f32[4]{0:T(128)S(1)} %dynamic_slice.7, bf16[512,4,128]{2,0,1:T(8,128)(2,1)S(1)} %fusion.26, bf16[512,128]{1,0:T(8,128)(2,1)} %fusion.29), kind=kOutput, calls=%fused_computation.71 | convolution fusion | flops 69990400 | bytes 2499072 | tf_op jit(solution)/shard_map/qhd,kd->hqk/dot_general | solution.py:73
  94.1 0.7 convolution_add_fusion.1
  94.7 0.0 copy-start.3
  94.7 0.0 copy-start.6
  94.8 0.0 copy-start.9
  94.8 0.8 fusion.22
  95.6 1.0 fusion.13
  96.5 0.0 copy-done.3
  96.5 0.0 copy-done.6
  96.6 0.0 copy-done.9
  96.6 3.1 %bitcast_reduce_fusion = (f32[4,256,4]{1,2,0:T(4,128)S(1)}, f32[4,256,512]{1,2,0:T(8,128)}, f32[512,256,4]{1,0,2:T(8,128)S(1)}) fusion(f32[4]{0:T(128)S(1)} %dynamic_slice.7, pred[256,512]{0,1:T(8,128)(4,1)S(1)} %copy-done.3, bf16[512,4,128]{2,0,1:T(8,128)(2,1)S(1)} %copy-done.6, bf16[512,128]{1,0:T(8,128)(2,1)S(1)} %copy-done.9), kind=kOutput, calls=%fused_computation.70 | convolution fusion | flops 139980800 | bytes 4735488 | tf_op jit(solution)/shard_map/qhd,kd->hqk/dot_general | solution.py:73
  99.6 0.1 reduce_window_sum.21
  99.7 0.0 copy-start.4
  99.7 2.9 %convolution_add_fusion = f32[4,256,4,128]{1,3,2,0:T(8,128)S(1)} fusion(f32[4,256,4,128]{1,3,2,0:T(8,128)} %bitcast.99, f32[4,256,4]{1,2,0:T(4,128)S(1)} %sub.15), kind=kOutput, calls=%fused_computation.19 | convolution fusion | flops 805847040 | bytes 4210688 | tf_op jit(solution)/shard_map/hqbk,kj->hqbj/dot_general | solution.py:31
  102.6 0.0 copy-done.4
  102.6 0.0 copy-start.2
  102.6 1.8 %fusion.4 = bf16[4,256,512]{1,2,0:T(8,128)(2,1)S(1)} fusion(f32[4,256,4,128]{1,3,2,0:T(8,128)S(1)} %convolution_add_fusion, f32[512,256,4]{1,0,2:T(8,128)S(1)} %get-tuple-element.9, f32[4]{0:T(128)S(1)} %dynamic_slice.7, pred[256,512]{0,1:T(8,128)(4,1)S(1)} %copy-done.4), kind=kLoop, calls=%fused_computation.8 | loop fusion | flops 6815744 | bytes 5373968 | tf_op jit(solution)/shard_map/convert_element_type | solution.py:80
  104.4 0.3 fusion.14
  104.7 0.0 copy-done.2
  104.8 0.1 convert_element_type.55
  104.9 0.1 copy.66
  105.0 11.2 %all_to_all.28 = bf16[4,128,512]{1,2,0:T(8,128)(2,1)S(1)} all-to-all(bf16[4,128,512]{1,2,0:T(8,128)(2,1)S(1)} %copy.66), channel_id=1, replica_groups=mesh['sp'=4,'dp'=8] {'sp'}, dimensions={0} | all-to-all | bytes 1048576 | tf_op jit(solution)/shard_map/all_to_all | solution.py:91
  116.2 1.0 copy.67
  (11 shorter events, 0.2 us)
Async XLA Ops:
  6.5 1.2 copy-start
  6.5 5.6 %copy-start.7 = (bf16[1,128,512]{2,1,0:T(8,128)(2,1)S(1)}, bf16[1,128,512]{2,1,0:T(8,128)(2,1)}, u32[]{:S(2)}) copy-start(bf16[1,128,512]{2,1,0:T(8,128)(2,1)} %param.12) | copy-start | bytes 393220
  6.5 5.8 %copy-start.8 = (bf16[1,128,512]{2,1,0:T(8,128)(2,1)S(1)}, bf16[1,128,512]{2,1,0:T(8,128)(2,1)}, u32[]{:S(2)}) copy-start(bf16[1,128,512]{2,1,0:T(8,128)(2,1)} %param.14) | copy-start | bytes 393220
  6.5 55.5 %all-gather.6.cloned.1.call-start = ((), (), s32[]{:S(2)}) async-start(), calls=%async_computation.3 | async-start | bytes 2433024 | tf_op jit(solution)/shard_map/all_gather | solution.py:57
  8.5 9.1 %copy-start.12 = (f32[16]{0:T(128)S(1)}, f32[16]{0:T(128)}, u32[]{:S(2)}) copy-start(f32[16]{0:T(128)} %param.15) | copy-start | bytes 196
  8.5 76.5 %all-gather.4.cloned.1.call-start = ((), (), s32[]{:S(2)}) async-start(), calls=%async_computation.2 | async-start | bytes 2641920 | tf_op jit(solution)/shard_map/all_gather | solution.py:59
  9.9 13.9 %copy-start.10 = (f32[128]{0:T(128)S(1)}, f32[128]{0:T(128)}, u32[]{:S(2)}) copy-start(f32[128]{0:T(128)} %param.13) | copy-start | bytes 1540
  13.3 10.3 %all-to-all-start = ((bf16[128,2,4,128]{3,0,1,2:T(8,128)(2,1)}), bf16[128,2,4,128]{3,0,1,2:T(8,128)(2,1)S(1)}, u32[]{:S(2)}, u32[]{:S(2)}) async-start(bf16[128,2,4,128]{3,0,1,2:T(8,128)(2,1)} %copy.56), calls=%async_computation | async-start | bytes 524288 | tf_op jit(solution)/shard_map/all_to_all | solution.py:51
  88.9 2.2 %copy-start.1 = (bf16[512,512]{1,0:T(8,128)(2,1)S(1)}, bf16[512,512]{1,0:T(8,128)(2,1)}, u32[]{:S(2)}) copy-start(bf16[512,512]{1,0:T(8,128)(2,1)} %convolution_convert_fusion) | copy-start | bytes 1572868
  88.9 2.2 %copy-start.11 = (f32[128]{0:T(128)S(1)}, f32[128]{0:T(128)}, u32[]{:S(2)}) copy-start(f32[128]{0:T(128)} %param.11) | copy-start | bytes 1540
  91.4 0.8 copy-start.5
  94.7 1.8 %copy-start.3 = (pred[256,512]{0,1:T(8,128)(4,1)S(1)}, pred[256,512]{0,1:T(8,128)(4,1)}, u32[]{:S(2)}) copy-start(pred[256,512]{0,1:T(8,128)(4,1)} %iota_compare_fusion) | copy-start | bytes 393220
  94.7 1.8 %copy-start.6 = (bf16[512,4,128]{2,0,1:T(8,128)(2,1)S(1)}, bf16[512,4,128]{2,0,1:T(8,128)(2,1)}, u32[]{:S(2)}) copy-start(bf16[512,4,128]{2,0,1:T(8,128)(2,1)} %copy-done.5) | copy-start | bytes 1572868
  94.8 1.8 %copy-start.9 = (bf16[512,128]{1,0:T(8,128)(2,1)S(1)}, bf16[512,128]{1,0:T(8,128)(2,1)}, u32[]{:S(2)}) copy-start(bf16[512,128]{1,0:T(8,128)(2,1)} %fusion.29) | copy-start | bytes 393220
  99.7 2.9 %copy-start.4 = (pred[256,512]{0,1:T(8,128)(4,1)S(1)}, pred[256,512]{0,1:T(8,128)(4,1)}, u32[]{:S(2)}) copy-start(pred[256,512]{0,1:T(8,128)(4,1)} %iota_compare_fusion) | copy-start | bytes 393220
  102.6 2.1 %copy-start.2 = (bf16[256,4,128]{0,2,1:T(8,128)(2,1)S(1)}, bf16[256,4,128]{0,2,1:T(8,128)(2,1)}, u32[]{:S(2)}) copy-start(bf16[256,4,128]{0,2,1:T(8,128)(2,1)} %fusion.13) | copy-start | bytes 786436
Sparse Core Ops, SparseCore 0:
  9.5 52.5 all-gather.5
  63.6 21.4 all-gather.3
where the time goes:
time: 125 us; the launch traced here: 124 us
  waiting for transfers between devices  63.8 us (51%)
  between operations  13.7 us (11%)
  matrix products  13.5 us (11%)
  blocking collectives  11.2 us (9%)
  other arithmetic  9.01 us (7%)
  local copies, waits for them, and re-layouts  8.58 us (7%)
  starting transfers between devices  4.31 us (3%)
    all_gather x1, waiting for transfers between devices, body(): gathered = lax.all_gather(columns, 'dp', axis=0, tiled=True)  37.5 us
    all_gather x1, waiting for transfers between devices, body(): lax.all_gather(normed, 'sp', axis=0, tiled=True)  21.1 us
    all_to_all x1, blocking collectives, body(): lax.all_to_all(attended, 'sp', split_axis=0, concat_axis=1, tiled=True)  11.2 us
    all_to_all x1, waiting for transfers between devices, body(): lax.all_to_all(copied, 'sp', split_axis=2, concat_axis=0, tiled=True)  5.16 us
    unnamed x30, local copies, waits for them, and re-layouts  4.87 us
    dot_general x2, matrix products, body(): jnp.einsum('qhd,kd->hqk', mine[first:finish], key_heads[:finish], preferr...  4.85 us
    all_to_all x1, starting transfers between devices, body(): lax.all_to_all(copied, 'sp', split_axis=2, concat_axis=0, tiled=True)  4.26 us
    dot_general x1, matrix products, body(): jnp.dot(lax.all_gather(normed, 'sp', axis=0, tiled=True), gathered, prefe...  3.8 us
  transfers between devices with their start and end apart: 3, of which 3 were waited for; matrix products, arithmetic and copies ran while one was open for 7% of the time, Pallas kernels for 0%

commit v1 on v0

--- a/solution.py
+++ b/solution.py
@@ -54,7 +54,12 @@
     columns = lax.dynamic_slice_in_dim(
         query_weight, sp_index * (heads_dev * head_width), heads_dev * head_width, 1
     )
-    gathered = lax.all_gather(columns, "dp", axis=0, tiled=True)
+    ring = [columns]
+    for hop in range(7):
+        ring.append(lax.ppermute(ring[-1], "dp", [(dev, (dev + 1) % 8) for dev in range(8)]))
+    gathered = jnp.roll(
+        jnp.concatenate(ring[::-1], axis=0), (lax.axis_index("dp") + 1) * ring[0].shape[0], axis=0
+    )
     queries = jnp.dot(
         lax.all_gather(normed, "sp", axis=0, tiled=True),
         gathered,

time: 125 us -> 152 us (1.22)
  local copies, waits for them, and re-layouts: 8.58 us -> 38 us
  waiting for transfers between devices: 63.8 us -> 58.1 us
  starting transfers between devices: 4.31 us -> 7.07 us
    ppermute x0 -> x7, waiting for transfers between devices: none -> 56.9 us  [body(): lax.ppermute(ring[-1], 'dp', [(dev, (dev + 1) % 8) for dev in range(8)])]
    all_gather x1 -> x0, waiting for transfers between devices: 37.5 us -> none  [body(): gathered = lax.all_gather(columns, 'dp', axis=0, tiled=True)]
    concatenate x0 -> x1, local copies, waits for them, and re-layouts: none -> 33.4 us  [body(): jnp.roll(jnp.concatenate(ring[::-1], axis=0), (lax.axis_index('dp') + 1)...]
    all_gather x1, waiting for transfers between devices: 21.1 us -> 0.01 us  [body(): lax.all_gather(normed, 'sp', axis=0, tiled=True)]
    all_to_all x1, waiting for transfers between devices: 5.16 us -> 1.26 us  [body(): lax.all_to_all(copied, 'sp', split_axis=2, concat_axis=0, tiled=True)]
    unnamed x30 -> x26, local copies, waits for them, and re-layouts: 4.87 us -> 1.07 us
    ppermute x0 -> x7, starting transfers between devices: none -> 3.04 us  [body(): lax.ppermute(ring[-1], 'dp', [(dev, (dev + 1) % 8) for dev in range(8)])]
  transfers between devices with their start and end apart: 3 -> 9, of which waited for: 3 -> 8; matrix products, arithmetic and copies ran while one was open for 7% -> 25% of each run, Pallas kernels for 0% -> 0%
where the time goes in v1:
time: 152 us; the launch traced here: 151 us
  waiting for transfers between devices  58.1 us (38%)
  local copies, waits for them, and re-layouts  38 us (25%)
  between operations  13.7 us (9%)
  matrix products  13.3 us (9%)
  blocking collectives  11.2 us (7%)
  other arithmetic  9.08 us (6%)
  starting transfers between devices  7.07 us (5%)
    ppermute x7, waiting for transfers between devices, body(): lax.ppermute(ring[-1], 'dp', [(dev, (dev + 1) % 8) for dev in range(8)])  56.9 us
    concatenate x1, local copies, waits for them, and re-layouts, body(): jnp.roll(jnp.concatenate(ring[::-1], axis=0), (lax.axis_index('dp') + 1)...  33.4 us
    all_to_all x1, blocking collectives, body(): lax.all_to_all(attended, 'sp', split_axis=0, concat_axis=1, tiled=True)  11.2 us
    dot_general x2, matrix products, body(): jnp.einsum('qhd,kd->hqk', mine[first:finish], key_heads[:finish], preferr...  4.84 us
    all_to_all x1, starting transfers between devices, body(): lax.all_to_all(copied, 'sp', split_axis=2, concat_axis=0, tiled=True)  4.03 us
    dot_general x1, matrix products, body(): jnp.dot(lax.all_gather(normed, 'sp', axis=0, tiled=True), gathered, prefe...  3.65 us
    dot_general x2, matrix products, stick_weights(): jnp.einsum('hqbk,kj->hqbj', pieces, upper, precision=lax.Precision.HIGHEST)  3.53 us
    convert_element_type x3, other arithmetic, rms_scaled(): return scaled.astype(jnp.bfloat16)  3.34 us
  transfers between devices with their start and end apart: 9, of which 8 were waited for; matrix products, arithmetic and copies ran while one was open for 25% of the time, Pallas kernels for 0%

profile of v1, /device:TPU:0, one launch (start us, length us, event | category | flops | bytes accessed | tf_op | source)
XLA Modules:
  0.0 150.5 jit_solution(10587345647000402010)
XLA Ops:
  6.5 0.0 copy-start
  6.5 0.0 all-gather.2.cloned.1.call-start
  6.5 1.4 fusion.20
  8.0 2.2 %fusion.22 = bf16[128,2064]{0,1:T(8,128)(2,1)} fusion(bf16[1,128,2064]{1,2,0:T(8,128)(2,1)} %param.8, f32[2064]{0:T(1024)} %param.9, f32[128]{0:T(128)S(1)} %add_rsqrt_fusion.2), kind=kLoop, calls=%fused_computation.35 | loop fusion | flops 1056768 | bytes 1065536 | tf_op jit(solution)/shard_map/convert_element_type | solution.py:15
  10.2 0.0 all-gather.2.cloned.1.call-update
  10.2 0.0 copy-done
  10.3 3.0 %collective-permute-start = (bf16[258,512]{1,0:T(8,128)(2,1)S(1)}, bf16[258,512]{1,0:T(8,128)(2,1)S(1)}, u32[]{:S(2)}, u32[]{:S(2)}) collective-permute-start(bf16[258,512]{1,0:T(8,128)(2,1)S(1)} %constant_dynamic-slice_fusion), channel_id=1, source_target_pairs={{0,1},{1,2},{2,3},{3,4},{4,5},{5,6},{6,7},{7,0},{8,9},{9,10},{10,1... | collective-permute-start | bytes 792584 | tf_op jit(solution)/shard_map/ppermute | solution.py:59
  13.3 9.5 %collective-permute-done = bf16[258,512]{1,0:T(8,128)(2,1)S(1)} collective-permute-done((bf16[258,512]{1,0:T(8,128)(2,1)S(1)}, bf16[258,512]{1,0:T(8,128)(2,1)S(1)}, u32[]{:S(2)}, u32[]{:S(2)}) %collective-permute-start) | collective-permute-done | bytes 264224 | tf_op jit(solution)/shard_map/ppermute | solution.py:59
  22.8 0.0 collective-permute-start.1
  22.8 10.3 %collective-permute-done.1 = bf16[258,512]{1,0:T(8,128)(2,1)S(1)} collective-permute-done((bf16[258,512]{1,0:T(8,128)(2,1)S(1)}, bf16[258,512]{1,0:T(8,128)(2,1)S(1)}, u32[]{:S(2)}, u32[]{:S(2)}) %collective-permute-start.1) | collective-permute-done | bytes 264224 | tf_op jit(solution)/shard_map/ppermute | solution.py:59
  33.2 0.0 collective-permute-start.2
  33.2 9.5 %collective-permute-done.2 = bf16[258,512]{1,0:T(8,128)(2,1)S(1)} collective-permute-done((bf16[258,512]{1,0:T(8,128)(2,1)S(1)}, bf16[258,512]{1,0:T(8,128)(2,1)S(1)}, u32[]{:S(2)}, u32[]{:S(2)}) %collective-permute-start.2) | collective-permute-done | bytes 264224 | tf_op jit(solution)/shard_map/ppermute | solution.py:59
  42.7 0.0 collective-permute-start.3
  42.7 9.2 %collective-permute-done.3 = bf16[258,512]{1,0:T(8,128)(2,1)S(1)} collective-permute-done((bf16[258,512]{1,0:T(8,128)(2,1)S(1)}, bf16[258,512]{1,0:T(8,128)(2,1)S(1)}, u32[]{:S(2)}, u32[]{:S(2)}) %collective-permute-start.3) | collective-permute-done | bytes 264224 | tf_op jit(solution)/shard_map/ppermute | solution.py:59
  51.8 0.0 collective-permute-start.4
  51.8 0.0 copy-done.6
  51.8 0.1 copy.44
  51.9 0.0 copy-done.7
  52.0 0.1 copy.45
  52.1 0.8 copy.46
  53.0 4.0 %all-to-all-start = ((bf16[128,2,4,128]{3,0,1,2:T(8,128)(2,1)}), bf16[128,2,4,128]{3,0,1,2:T(8,128)(2,1)}, u32[]{:S(2)}, u32[]{:S(2)}) async-start(bf16[128,2,4,128]{3,0,1,2:T(8,128)(2,1)} %copy.46), calls=%async_computation | async-start | bytes 524288 | tf_op jit(solution)/shard_map/all_to_all | solution.py:51
  57.0 4.0 %collective-permute-done.4 = bf16[258,512]{1,0:T(8,128)(2,1)S(1)} collective-permute-done((bf16[258,512]{1,0:T(8,128)(2,1)S(1)}, bf16[258,512]{1,0:T(8,128)(2,1)S(1)}, u32[]{:S(2)}, u32[]{:S(2)}) %collective-permute-start.4) | collective-permute-done | bytes 264224 | tf_op jit(solution)/shard_map/ppermute | solution.py:59
  61.0 0.0 collective-permute-start.5
  61.0 0.7 iota_compare_fusion
  61.7 0.0 copy-done.11
  61.7 0.1 dynamic_slice.12
  61.8 1.3 all-to-all-done
  63.1 1.0 copy.47
  64.0 0.1 fusion.32
  64.2 5.9 %collective-permute-done.5 = bf16[258,512]{1,0:T(8,128)(2,1)S(1)} collective-permute-done((bf16[258,512]{1,0:T(8,128)(2,1)S(1)}, bf16[258,512]{1,0:T(8,128)(2,1)S(1)}, u32[]{:S(2)}, u32[]{:S(2)}) %collective-permute-start.5) | collective-permute-done | bytes 264224 | tf_op jit(solution)/shard_map/ppermute | solution.py:59
  70.1 0.0 collective-permute-start.6
  70.1 0.0 copy-done.9
  70.1 0.8 fusion.34
  70.9 8.5 %collective-permute-done.6 = bf16[258,512]{1,0:T(8,128)(2,1)} collective-permute-done((bf16[258,512]{1,0:T(8,128)(2,1)S(1)}, bf16[258,512]{1,0:T(8,128)(2,1)}, u32[]{:S(2)}, u32[]{:S(2)}) %collective-permute-start.6) | collective-permute-done | bytes 264224 | tf_op jit(solution)/shard_map/ppermute | solution.py:59
  79.4 33.4 %concatenate.11 = bf16[4128,512]{1,0:T(8,128)(2,1)} concatenate(bf16[258,512]{1,0:T(8,128)(2,1)} %collective-permute-done.6, bf16[258,512]{1,0:T(8,128)(2,1)S(1)} %collective-permute-done.5, bf16[258,512]{1,0:T(8,128)(2,1)S(1)} %collective-permute-done.4, bf16[258,512]{1,0:T(8,128)(2,1)S(1)} %collective-permute-done.3, bf16[258,512]{1,0:T(8,128)(2,1)S(1)} %collective-permute-done.2, ...), dimensions={0} | concatenate | bytes 8454144 | tf_op jit(solution)/shard_map/jit(_roll_dynamic)/concatenate | solution.py:60
  112.8 3.7 %fusion.15 = bf16[512,512]{1,0:T(8,128)(2,1)S(1)} fusion(bf16[512,2064]{0,1:T(8,128)(2,1)} %all-gather.2.cloned.1.call-done, bf16[4128,512]{1,0:T(8,128)(2,1)} %concatenate.11, s32[]{:T(128)S(6)} %select_n.51), kind=kOutput, calls=%fused_computation.28 | convolution fusion | flops 1082392576 | bytes 4751364 | tf_op jit(solution)/shard_map/dot_general | solution.py:63
  116.5 0.0 copy-start.10
  116.5 0.3 reshape.88
  116.8 0.6 multiply_reduce_fusion
  117.4 0.1 copy.48
  117.6 0.0 copy-done.10
  117.6 0.3 fusion.31
  117.9 0.0 copy-start.4
  117.9 0.8 copy-done.4
  118.7 1.8 %bitcast_reduce_fusion.1 = (f32[4,256,2]{1,2,0:T(2,128)S(1)}, f32[4,256,256]{1,2,0:T(8,128)S(1)}, f32[4,256,256]{1,2,0:T(8,128)S(1)}) fusion(pred[256,256]{0,1:T(8,128)(4,1)S(1)} %iota_compare_fusion.1, f32[4]{0:T(128)S(1)} %dynamic_slice.12, bf16[512,4,128]{2,0,1:T(8,128)(2,1)S(1)} %fusion.31, bf16[512,128]{1,0:T(8,128)(2,1)} %fusion.34), kind=kOutput, calls=%fused_computation.74 | convolution fusion | flops 69990400 | bytes 2499072 | tf_op jit(solution)/shard_map/qhd,kd->hqk/dot_general | solution.py:78
  120.5 0.7 convolution_add_fusion.1
  121.2 0.0 copy-start.2
  121.2 0.0 copy-start.5
  121.2 0.0 copy-start.8
  121.2 0.8 fusion.27
  122.0 1.0 fusion.18
  123.0 0.0 copy-done.2
  123.0 0.0 copy-done.5
  123.0 0.0 copy-done.8
  123.0 3.1 %bitcast_reduce_fusion = (f32[4,256,4]{1,2,0:T(4,128)S(1)}, f32[4,256,512]{1,2,0:T(8,128)}, f32[512,256,4]{1,0,2:T(8,128)S(1)}) fusion(f32[4]{0:T(128)S(1)} %dynamic_slice.12, pred[256,512]{0,1:T(8,128)(4,1)S(1)} %copy-done.2, bf16[512,4,128]{2,0,1:T(8,128)(2,1)S(1)} %copy-done.5, bf16[512,128]{1,0:T(8,128)(2,1)S(1)} %copy-done.8), kind=kOutput, calls=%fused_computation.73 | convolution fusion | flops 139980800 | bytes 4735488 | tf_op jit(solution)/shard_map/qhd,kd->hqk/dot_general | solution.py:78
  126.1 0.1 reduce_window_sum.21
  126.1 0.0 copy-start.3
  126.2 2.9 %convolution_add_fusion = f32[4,256,4,128]{1,3,2,0:T(8,128)S(1)} fusion(f32[4,256,4,128]{1,3,2,0:T(8,128)} %bitcast.96, f32[4,256,4]{1,2,0:T(4,128)S(1)} %sub.20), kind=kOutput, calls=%fused_computation.21 | convolution fusion | flops 805847040 | bytes 4210688 | tf_op jit(solution)/shard_map/hqbk,kj->hqbj/dot_general | solution.py:31
  129.1 1.8 %fusion.6 = bf16[4,256,512]{1,2,0:T(8,128)(2,1)S(1)} fusion(f32[4,256,4,128]{1,3,2,0:T(8,128)S(1)} %convolution_add_fusion, f32[512,256,4]{1,0,2:T(8,128)S(1)} %get-tuple-element.9, f32[4]{0:T(128)S(1)} %dynamic_slice.12, pred[256,512]{0,1:T(8,128)(4,1)S(1)} %copy-done.3), kind=kLoop, calls=%fused_computation.10 | loop fusion | flops 6815744 | bytes 5373968 | tf_op jit(solution)/shard_map/convert_element_type | solution.py:85
  130.9 0.3 fusion.19
  131.2 0.1 convert_element_type.55
  131.4 0.1 copy.56
  131.5 11.2 %all_to_all.28 = bf16[4,128,512]{1,2,0:T(8,128)(2,1)S(1)} all-to-all(bf16[4,128,512]{1,2,0:T(8,128)(2,1)S(1)} %copy.56), channel_id=1, replica_groups=mesh['sp'=4,'dp'=8] {'sp'}, dimensions={0} | all-to-all | bytes 1048576 | tf_op jit(solution)/shard_map/all_to_all | solution.py:96
  142.7 1.0 copy.57
  (19 shorter events, 0.2 us)
Async XLA Ops:
  6.5 3.7 %copy-start = (bf16[258,2048]{1,0:T(8,128)(2,1)S(1)}, bf16[258,2048]{1,0:T(8,128)(2,1)}, u32[]{:S(2)}) copy-start(bf16[258,2048]{1,0:T(8,128)(2,1)} %param.10) | copy-start | bytes 3170308
  6.5 45.3 %copy-start.6 = (bf16[1,128,512]{2,1,0:T(8,128)(2,1)S(1)}, bf16[1,128,512]{2,1,0:T(8,128)(2,1)}, u32[]{:S(2)}) copy-start(bf16[1,128,512]{2,1,0:T(8,128)(2,1)} %param.12) | copy-start | bytes 393220
  6.5 45.4 %copy-start.7 = (bf16[1,128,512]{2,1,0:T(8,128)(2,1)S(1)}, bf16[1,128,512]{2,1,0:T(8,128)(2,1)}, u32[]{:S(2)}) copy-start(bf16[1,128,512]{2,1,0:T(8,128)(2,1)} %param.14) | copy-start | bytes 393220
  6.5 106.3 %all-gather.2.cloned.1.call-start = ((), (), s32[]{:S(2)}) async-start(), calls=%async_computation.2 | async-start | bytes 2641920 | tf_op jit(solution)/shard_map/all_gather | solution.py:64
  8.0 53.7 %copy-start.11 = (f32[16]{0:T(128)S(1)}, f32[16]{0:T(128)}, u32[]{:S(2)}) copy-start(f32[16]{0:T(128)} %param.15) | copy-start | bytes 196
  10.2 59.9 %copy-start.9 = (f32[128]{0:T(128)S(1)}, f32[128]{0:T(128)}, u32[]{:S(2)}) copy-start(f32[128]{0:T(128)} %param.13) | copy-start | bytes 1540
  10.3 12.5 %collective-permute-start = (bf16[258,512]{1,0:T(8,128)(2,1)S(1)}, bf16[258,512]{1,0:T(8,128)(2,1)S(1)}, u32[]{:S(2)}, u32[]{:S(2)}) collective-permute-start(bf16[258,512]{1,0:T(8,128)(2,1)S(1)} %constant_dynamic-slice_fusion), channel_id=1, source_target_pairs={{0,1},{1,2},{2,3},{3,4},{4,5},{5,6},{6,7},{7,0},{8,9},{9,10},{10,1... | collective-permute-start | bytes 792584 | tf_op jit(solution)/shard_map/ppermute | solution.py:59
  22.8 10.3 %collective-permute-start.1 = (bf16[258,512]{1,0:T(8,128)(2,1)S(1)}, bf16[258,512]{1,0:T(8,128)(2,1)S(1)}, u32[]{:S(2)}, u32[]{:S(2)}) collective-permute-start(bf16[258,512]{1,0:T(8,128)(2,1)S(1)} %collective-permute-done), channel_id=1, source_target_pairs={{0,1},{1,2},{2,3},{3,4},{4,5},{5,6},{6,7},{7,0},{8,9},{9,10},{10,1... | collective-permute-start | bytes 792584 | tf_op jit(solution)/shard_map/ppermute | solution.py:59
  33.2 9.5 %collective-permute-start.2 = (bf16[258,512]{1,0:T(8,128)(2,1)S(1)}, bf16[258,512]{1,0:T(8,128)(2,1)S(1)}, u32[]{:S(2)}, u32[]{:S(2)}) collective-permute-start(bf16[258,512]{1,0:T(8,128)(2,1)S(1)} %collective-permute-done.1), channel_id=1, source_target_pairs={{0,1},{1,2},{2,3},{3,4},{4,5},{5,6},{6,7},{7,0},{8,9},{9,10},{10,1... | collective-permute-start | bytes 792584 | tf_op jit(solution)/shard_map/ppermute | solution.py:59
  42.7 9.2 %collective-permute-start.3 = (bf16[258,512]{1,0:T(8,128)(2,1)S(1)}, bf16[258,512]{1,0:T(8,128)(2,1)S(1)}, u32[]{:S(2)}, u32[]{:S(2)}) collective-permute-start(bf16[258,512]{1,0:T(8,128)(2,1)S(1)} %collective-permute-done.2), channel_id=1, source_target_pairs={{0,1},{1,2},{2,3},{3,4},{4,5},{5,6},{6,7},{7,0},{8,9},{9,10},{10,1... | collective-permute-start | bytes 792584 | tf_op jit(solution)/shard_map/ppermute | solution.py:59
  51.8 9.2 %collective-permute-start.4 = (bf16[258,512]{1,0:T(8,128)(2,1)S(1)}, bf16[258,512]{1,0:T(8,128)(2,1)S(1)}, u32[]{:S(2)}, u32[]{:S(2)}) collective-permute-start(bf16[258,512]{1,0:T(8,128)(2,1)S(1)} %collective-permute-done.3), channel_id=1, source_target_pairs={{0,1},{1,2},{2,3},{3,4},{4,5},{5,6},{6,7},{7,0},{8,9},{9,10},{10,1... | collective-permute-start | bytes 792584 | tf_op jit(solution)/shard_map/ppermute | solution.py:59
  53.0 10.1 %all-to-all-start = ((bf16[128,2,4,128]{3,0,1,2:T(8,128)(2,1)}), bf16[128,2,4,128]{3,0,1,2:T(8,128)(2,1)}, u32[]{:S(2)}, u32[]{:S(2)}) async-start(bf16[128,2,4,128]{3,0,1,2:T(8,128)(2,1)} %copy.46), calls=%async_computation | async-start | bytes 524288 | tf_op jit(solution)/shard_map/all_to_all | solution.py:51
  61.0 9.2 %collective-permute-start.5 = (bf16[258,512]{1,0:T(8,128)(2,1)S(1)}, bf16[258,512]{1,0:T(8,128)(2,1)S(1)}, u32[]{:S(2)}, u32[]{:S(2)}) collective-permute-start(bf16[258,512]{1,0:T(8,128)(2,1)S(1)} %collective-permute-done.4), channel_id=1, source_target_pairs={{0,1},{1,2},{2,3},{3,4},{4,5},{5,6},{6,7},{7,0},{8,9},{9,10},{10,1... | collective-permute-start | bytes 792584 | tf_op jit(solution)/shard_map/ppermute | solution.py:59
  70.1 9.3 %collective-permute-start.6 = (bf16[258,512]{1,0:T(8,128)(2,1)S(1)}, bf16[258,512]{1,0:T(8,128)(2,1)}, u32[]{:S(2)}, u32[]{:S(2)}) collective-permute-start(bf16[258,512]{1,0:T(8,128)(2,1)S(1)} %collective-permute-done.5), channel_id=1, source_target_pairs={{0,1},{1,2},{2,3},{3,4},{4,5},{5,6},{6,7},{7,0},{8,9},{9,10},{10,1... | collective-permute-start | bytes 792584 | tf_op jit(solution)/shard_map/ppermute | solution.py:59
  116.5 1.1 copy-start.10
  117.9 0.8 copy-start.4
  121.2 1.8 %copy-start.2 = (pred[256,512]{0,1:T(8,128)(4,1)S(1)}, pred[256,512]{0,1:T(8,128)(4,1)}, u32[]{:S(2)}) copy-start(pred[256,512]{0,1:T(8,128)(4,1)} %iota_compare_fusion) | copy-start | bytes 393220
  121.2 1.8 %copy-start.5 = (bf16[512,4,128]{2,0,1:T(8,128)(2,1)S(1)}, bf16[512,4,128]{2,0,1:T(8,128)(2,1)}, u32[]{:S(2)}) copy-start(bf16[512,4,128]{2,0,1:T(8,128)(2,1)} %copy-done.4) | copy-start | bytes 1572868
  121.2 1.8 %copy-start.8 = (bf16[512,128]{1,0:T(8,128)(2,1)S(1)}, bf16[512,128]{1,0:T(8,128)(2,1)}, u32[]{:S(2)}) copy-start(bf16[512,128]{1,0:T(8,128)(2,1)} %fusion.34) | copy-start | bytes 393220
  126.1 2.9 %copy-start.3 = (pred[256,512]{0,1:T(8,128)(4,1)S(1)}, pred[256,512]{0,1:T(8,128)(4,1)}, u32[]{:S(2)}) copy-start(pred[256,512]{0,1:T(8,128)(4,1)} %iota_compare_fusion) | copy-start | bytes 393220
  129.0 2.1 %copy-start.1 = (bf16[256,4,128]{0,2,1:T(8,128)(2,1)S(1)}, bf16[256,4,128]{0,2,1:T(8,128)(2,1)}, u32[]{:S(2)}) copy-start(bf16[256,4,128]{0,2,1:T(8,128)(2,1)} %fusion.18) | copy-start | bytes 786436
Sparse Core Ops, SparseCore 0:
  10.4 25.6 all-gather.1
